TPU v7x, 32 devices: a whole 2x2x4 slice. The times are simulated.
32 devices in a mesh: sp: 8 (over z, x), tp: 4 (over y, core).
Axes of the slice: x: 2, y: 2, z: 4, core: 2. Of those that a mesh axis runs over, the one named last changes fastest.
Arguments:
- saved_tokens: bfloat16 [1536, 2048], P('sp'), may hold values from -3.75 to 3.75
- cotangent: bfloat16 [1536, 2048], P('sp'), may hold values from -6 to 6
- routes: int32 [1536, 2], P('sp'), may hold values from 0 to 7, all different within a row; in each aligned block of 192 rows (0 to 191, 192 to 383, ...) at most 96 rows name the same one
- route_weights: float32 [1536, 2], P('sp'), may hold values from 0.2 to 1
- gate_in: bfloat16 [1536, 1024], P('sp', 'tp'), may hold values from -6 to 6
- conv_in: bfloat16 [1536, 1024], P('sp', 'tp'), may hold values from -6 to 6
- value_in: bfloat16 [1536, 1024], P('sp', 'tp'), may hold values from -6 to 6
- conv_taps: float32 [3, 1024], replicated, may hold values from -3.5 to 3.5
- out_weight: bfloat16 [2048, 1024], P(None, 'tp'), may hold values from -0.1875 to 0.1875
- gate_proj: bfloat16 [8, 2048, 2048], P('sp', None, 'tp'), may hold values from -0.125 to 0.125
- up_proj: bfloat16 [8, 2048, 2048], P('sp', None, 'tp'), may hold values from -0.125 to 0.125
- down_proj: bfloat16 [8, 2048, 2048], P('sp', 'tp'), may hold values from -0.125 to 0.125
Outputs:
- gate_proj_grad: float32 [8, 2048, 2048], P('sp', None, 'tp')
- up_proj_grad: float32 [8, 2048, 2048], P('sp', None, 'tp')
- down_proj_grad: float32 [8, 2048, 2048], P('sp', 'tp')
- out_weight_grad: float32 [2048, 1024], P('sp', 'tp')
- token_grad: bfloat16 [1536, 2048], P('sp', 'tp')
- gate_in_grad: bfloat16 [1536, 1024], P('sp', 'tp')
- conv_in_grad: bfloat16 [1536, 1024], P('sp', 'tp')
- value_in_grad: bfloat16 [1536, 1024], P('sp', 'tp')
Inputs may be any that keep to these rules, and one draw needn't show every extreme that they name: `routes`: within each aligned block of 192 tokens at most 96 assignments name one expert, a bound that some block reaches of them; the 2 experts of a token differ.
All inputs are finite; a program needn't handle non-finite values.
Results may differ from a plain program's by a relative error of at most 0.0063.
Values may be sent and summed in bfloat16 or wider, within the bound.
A program may use at most 64 MiB of HBM per device.

v0:
```python
import jax
import jax.numpy as jnp
from jax import lax
from jax.sharding import PartitionSpec as P

CLAMP_LIMIT = 7.0
SILU_ALPHA = 1.702


def padded(cells, sides, width):
    for axis, dim in sides:
        count = lax.axis_size(axis)
        ends = count - 1
        head = lax.slice_in_dim(cells, 0, width, axis=dim)
        tail = lax.slice_in_dim(cells, cells.shape[dim] - width, cells.shape[dim], axis=dim)
        cells = jnp.concatenate(
            [
                lax.ppermute(tail, axis, [(i, (i + 1) % count) for i in range(ends)]),
                cells,
                lax.ppermute(head, axis, [((i + 1) % count, i) for i in range(ends)]),
            ],
            axis=dim,
        )
    return cells


def contract_rows(left, right):
    return lax.dot_general(
        left, right, (((0,), (0,)), ((), ())), preferred_element_type=jnp.float32
    )


def contract_cols(left, right):
    return lax.dot_general(
        left, right, (((1,), (1,)), ((), ())), preferred_element_type=jnp.float32
    )


def expert_backward(rows_in, grads_in, w_gate, w_up, w_down):
    gate_pre = jnp.dot(rows_in, w_gate, preferred_element_type=jnp.float32)
    up_pre = jnp.dot(rows_in, w_up, preferred_element_type=jnp.float32)
    gate_clip = jnp.minimum(gate_pre, CLAMP_LIMIT)
    up_clip = jnp.clip(up_pre, -CLAMP_LIMIT, CLAMP_LIMIT)
    sigmoid_gate = jax.nn.sigmoid(SILU_ALPHA * gate_clip)
    gated_act = gate_clip * sigmoid_gate
    hidden = ((up_clip + 1.0) * gated_act).astype(jnp.bfloat16)
    d_hidden = contract_cols(grads_in, w_down)
    d_up = jnp.where(jnp.abs(up_pre) < CLAMP_LIMIT, d_hidden * gated_act, 0.0).astype(jnp.bfloat16)
    gate_slope = sigmoid_gate + SILU_ALPHA * gate_clip * sigmoid_gate * (1.0 - sigmoid_gate)
    d_gate = jnp.where(gate_pre < CLAMP_LIMIT, d_hidden * (up_clip + 1.0) * gate_slope, 0.0).astype(
        jnp.bfloat16
    )
    down_grad = contract_rows(hidden, grads_in)
    gate_grad = contract_rows(rows_in, d_gate)
    up_grad = contract_rows(rows_in, d_up)
    partial_value = contract_cols(d_gate, w_gate) + contract_cols(d_up, w_up)
    return (gate_grad, up_grad, down_grad, partial_value.astype(jnp.bfloat16))


def local(
    saved_tokens,
    cotangent,
    routes,
    route_weights,
    gate_in,
    conv_in,
    value_in,
    conv_taps,
    out_weight,
    gate_proj,
    up_proj,
    down_proj,
):
    tok_rows, model_width = saved_tokens.shape
    top_count = routes.shape[1]
    expert_count = lax.axis_size("sp")
    tp_count = lax.axis_size("tp")
    capacity = 2 * tok_rows * top_count // expert_count
    assigns = tok_rows * top_count
    part_width = model_width // tp_count
    offset = lax.axis_index("tp") * part_width
    flat_routes = routes.reshape(assigns)
    onehot = (flat_routes[:, None] == jnp.arange(expert_count, dtype=jnp.int32)[None, :]).astype(
        jnp.int32
    )
    slot_rank = jnp.sum((jnp.cumsum(onehot, axis=0) - 1) * onehot, axis=1)
    slot_index = flat_routes * capacity + slot_rank
    slot_owner = (
        jnp.full((expert_count * capacity,), assigns, jnp.int32)
        .at[slot_index]
        .set(jnp.arange(assigns, dtype=jnp.int32))
    )
    zero_row = jnp.zeros((1, model_width), jnp.bfloat16)
    token_rows = jnp.concatenate([saved_tokens, zero_row], 0)[slot_owner // top_count]
    scaled = (route_weights[:, :, None] * cotangent.astype(jnp.float32)[:, None, :]).astype(
        jnp.bfloat16
    )
    grad_rows = jnp.concatenate([scaled.reshape(assigns, model_width), zero_row], 0)[slot_owner]
    send_tokens = token_rows.reshape(expert_count, capacity, model_width)
    send_grads = grad_rows.reshape(expert_count, capacity, model_width)
    sliced = (
        lax.dynamic_slice_in_dim(send_tokens, offset, part_width, 2),
        lax.dynamic_slice_in_dim(send_grads, offset, part_width, 2),
    )
    arrived = (
        lax.all_to_all(sliced[0], "sp", split_axis=0, concat_axis=0, tiled=True),
        lax.all_to_all(sliced[1], "sp", split_axis=0, concat_axis=0, tiled=True),
    )
    recv_tokens, recv_grads = (
        lax.all_gather(arrived[0], "tp", axis=2, tiled=True),
        lax.all_gather(arrived[1], "tp", axis=2, tiled=True),
    )
    gate_grad, up_grad, down_grad, partial_value = expert_backward(
        recv_tokens.reshape(-1, model_width),
        recv_grads.reshape(-1, model_width),
        gate_proj[0],
        up_proj[0],
        down_proj[0],
    )
    grouped = partial_value.reshape(expert_count * capacity, tp_count, part_width)
    pieces = lax.all_to_all(grouped, "tp", split_axis=1, concat_axis=1, tiled=True)
    shares = jnp.sum(pieces.astype(jnp.float32), axis=1).reshape(expert_count, capacity, part_width)
    returned = lax.all_to_all(shares, "sp", split_axis=0, concat_axis=0, tiled=True)
    picked = returned.reshape(-1, part_width)[slot_index]
    combined = jnp.sum(picked.reshape(tok_rows, top_count, part_width), axis=1)
    own_cot = lax.dynamic_slice_in_dim(cotangent, offset, part_width, 1).astype(jnp.float32)
    token_grad = (own_cot + combined).astype(jnp.bfloat16)
    residual = lax.all_gather(token_grad, "tp", axis=1, tiled=True)
    channels = gate_in.shape[1]
    d_conv_out = jnp.dot(residual, out_weight, preferred_element_type=jnp.float32)
    gate_f32 = gate_in.astype(jnp.float32)
    conv_f32 = conv_in.astype(jnp.float32)
    value_f32 = value_in.astype(jnp.float32)
    product = conv_f32 * value_f32
    back_signal = d_conv_out * gate_f32
    rimmed = padded(jnp.concatenate([product, back_signal], 1), (("sp", 0),), 1)
    prod_rim = rimmed[:, :channels]
    grad_rim = rimmed[:, channels:]
    my_taps = lax.dynamic_slice_in_dim(conv_taps, lax.axis_index("tp") * channels, channels, 1)
    conv_out = my_taps[0] * prod_rim[:-2] + my_taps[1] * prod_rim[1:-1] + my_taps[2] * prod_rim[2:]
    d_product = my_taps[0] * grad_rim[2:] + my_taps[1] * grad_rim[1:-1] + my_taps[2] * grad_rim[:-2]
    gate_in_grad = (d_conv_out * conv_out).astype(jnp.bfloat16)
    conv_in_grad = (d_product * value_f32).astype(jnp.bfloat16)
    value_in_grad = (d_product * conv_f32).astype(jnp.bfloat16)
    mixed_act = (gate_f32 * conv_out).astype(jnp.bfloat16)
    out_weight_grad = lax.psum_scatter(
        contract_rows(residual, mixed_act), "sp", scatter_dimension=0, tiled=True
    )
    return (
        gate_grad[None],
        up_grad[None],
        down_grad[None],
        out_weight_grad,
        token_grad,
        gate_in_grad,
        conv_in_grad,
        value_in_grad,
    )


def solution(mesh):
    in_specs = (
        P("sp", None),
        P("sp", None),
        P("sp", None),
        P("sp", None),
        P("sp", "tp"),
        P("sp", "tp"),
        P("sp", "tp"),
        P(),
        P(None, "tp"),
        P("sp", None, "tp"),
        P("sp", None, "tp"),
        P("sp", "tp", None),
    )
    out_specs = (
        P("sp", None, "tp"),
        P("sp", None, "tp"),
        P("sp", "tp", None),
        P("sp", "tp"),
        P("sp", "tp"),
        P("sp", "tp"),
        P("sp", "tp"),
        P("sp", "tp"),
    )
    return jax.shard_map(local, mesh=mesh, in_specs=in_specs, out_specs=out_specs, check_vma=False)
```

profile of v0, /device:TPU:0, one launch (start us, length us, event | category | flops | bytes accessed | tf_op | source)
XLA Modules:
  0.0 314.1 jit_solution(3205792691582930578)
XLA Ops:
  10.7 2.9 scatter_custom_fusion
  14.8 4.2 %gather_fusion = bf16[768,2048]{1,0:T(8,128)(2,1)} fusion(bf16[193,2048]{1,0:T(8,128)(2,1)S(1)} %concatenate.18, s32[1024]{0:T(1024)S(1)} %get-tuple-element.22), kind=kCustom, calls=%fused_computation | custom fusion | bytes 6294528 | tf_op jit(solution)/shard_map/gather | solution.py:94
  20.3 27.3 %all_to_all.20 = bf16[8,96,512]{2,1,0:T(8,128)(2,1)} all-to-all(bf16[8,96,512]{2,1,0:T(8,128)(2,1)S(1)} %constant_dynamic-slice_fusion.2), channel_id=1, replica_groups=mesh['sp'=8,'tp'=4] {'sp'}, dimensions={0} | all-to-all | bytes 1572864 | tf_op jit(solution)/shard_map/all_to_all | solution.py:106
  47.7 3.3 %mul.141 = f32[192,2,2048]{2,1,0:T(2,128)} broadcast(bf16[192,2048]{1,0:T(8,128)(2,1)S(1)} %copy-done.3), dimensions={0,2} | broadcast | bytes 3932160 | tf_op jit(solution)/shard_map/mul | solution.py:95
  51.0 5.4 %mul.142 = f32[384,2048]{1,0:T(8,128)} reshape(f32[192,2,2048]{2,1,0:T(2,128)} %mul.141) | data formatting | bytes 6291456 | tf_op jit(solution)/shard_map/mul | solution.py:95
  56.7 2.1 multiply_convert_fusion
  60.1 8.7 %gather_fusion.1 = bf16[768,2048]{1,0:T(8,128)(2,1)} fusion(bf16[385,2048]{1,0:T(8,128)(2,1)} %concatenate.19, s32[1024]{0:T(1024)S(1)} %get-tuple-element.21), kind=kCustom, calls=%fused_computation.1 | custom fusion | bytes 6294528 | tf_op jit(solution)/shard_map/gather | solution.py:98
  70.0 23.4 %all_to_all.21 = bf16[8,96,512]{2,1,0:T(8,128)(2,1)} all-to-all(bf16[8,96,512]{2,1,0:T(8,128)(2,1)S(1)} %constant_dynamic-slice_fusion.1), channel_id=1, replica_groups=mesh['sp'=8,'tp'=4] {'sp'}, dimensions={0} | all-to-all | bytes 1572864 | tf_op jit(solution)/shard_map/all_to_all | solution.py:107
  93.5 5.6 %fusion.1 = f32[768,512]{1,0:T(8,128)} fusion(bf16[768,2048]{1,0:T(8,128)(2,1)} %bitcast.70, bf16[1,2048,512]{2,1,0:T(8,128)(2,1)} %param.22), kind=kOutput, calls=%fused_computation.12 | convolution fusion | flops 1610612736 | bytes 6815744 | tf_op jit(solution)/shard_map/dot_general | solution.py:41
  99.1 3.0 fusion.7
  102.1 19.1 %all-gather.5.cloned.1.call-done = bf16[8,96,2048]{2,1,0:T(8,128)(2,1)} async-done(((bf16[8,96,512]{2,1,0:T(8,128)(2,1)}), bf16[8,96,2048]{2,1,0:T(8,128)(2,1)}) %all-gather.5.cloned.1.call-update) | async-done | bytes 3145744 | tf_op jit(solution)/shard_map/all_gather | solution.py:111
  121.2 6.1 %select_convert_fusion = (bf16[768,512]{1,0:T(8,128)(2,1)S(1)}, bf16[768,512]{1,0:T(8,128)(2,1)S(1)}) fusion(f32[768,512]{1,0:T(8,128)} %fusion.1, f32[768,512]{1,0:T(8,128)} %fusion.7, bf16[768,2048]{1,0:T(8,128)(2,1)} %bitcast.74, bf16[1,512,2048]{2,1,0:T(8,128)(2,1)} %param.23), kind=kOutput, calls=%fused_computation.21 | convolution fusion | flops 1619263488 | bytes 9961472 | tf_op jit(solution)/shard_map/dot_general | solution.py:34
  129.6 1.8 add_convert_fusion
  131.7 39.4 %all_to_all.22 = bf16[768,4,512]{2,0,1:T(8,128)(2,1)S(1)} all-to-all(bf16[768,4,512]{2,0,1:T(8,128)(2,1)S(1)} %bitcast.55), channel_id=1, replica_groups=mesh['sp'=8,'tp'=4] {'tp'}, dimensions={1} | all-to-all | bytes 6291456 | tf_op jit(solution)/shard_map/all_to_all | solution.py:121
  172.8 5.6 %all-to-all-start.3 = ((f32[8,96,512]{2,1,0:T(8,128)}), f32[8,96,512]{2,1,0:T(8,128)S(1)}, u32[]{:S(2)}, u32[]{:S(2)}) async-start(f32[8,96,512]{2,1,0:T(8,128)} %bitcast.57), calls=%async_computation.3 | async-start | bytes 3145728 | tf_op jit(solution)/shard_map/all_to_all | solution.py:123
  178.5 36.5 %all-to-all-done.3 = f32[8,96,512]{2,1,0:T(8,128)S(1)} async-done(((f32[8,96,512]{2,1,0:T(8,128)}), f32[8,96,512]{2,1,0:T(8,128)S(1)}, u32[]{:S(2)}, u32[]{:S(2)}) %all-to-all-start.3) | async-done | bytes 1572896 | tf_op jit(solution)/shard_map/all_to_all | solution.py:123
  219.8 7.9 %all_gather.11 = bf16[192,2048]{1,0:T(8,128)(2,1)S(1)} all-gather(bf16[192,512]{1,0:T(8,128)(2,1)S(1)} %add_convert_fusion.1), channel_id=1, replica_groups=mesh['sp'=8,'tp'=4] {'tp'}, dimensions={1}, use_global_device_ids=true | all-gather | bytes 983040 | tf_op jit(solution)/shard_map/all_gather | solution.py:128
  228.8 3.3 %collective-permute-start = (f32[1,512]{1,0:T(1,128)S(1)}, f32[1,512]{1,0:T(1,128)S(1)}, u32[]{:S(2)}, u32[]{:S(2)}) collective-permute-start(f32[1,512]{1,0:T(1,128)S(1)} %get-tuple-element.12), channel_id=1, source_target_pairs={{0,4},{4,8},{8,12},{12,16},{16,20},{20,24},{24,28},{1,5},{5,9},{9,... | collective-permute-start | bytes 6152 | tf_op jit(solution)/shard_map/ppermute | solution.py:18
  234.5 3.1 collective-permute-done.1
  237.6 1.9 fusion.21
  239.5 5.9 %convolution_bitcast_fusion.1 = f32[1,2048,512]{2,1,0:T(8,128)} fusion(bf16[768,2048]{1,0:T(8,128)(2,1)} %bitcast.71, bf16[768,512]{1,0:T(8,128)(2,1)S(1)} %copy-done.8), kind=kOutput, calls=%fused_computation.7 | convolution fusion | flops 1610612736 | bytes 8126464 | tf_op jit(solution)/shard_map/dot_general | solution.py:28
  245.4 3.9 %convolution_bitcast_fusion.2 = f32[1,2048,512]{2,1,0:T(8,128)} fusion(bf16[768,2048]{1,0:T(8,128)(2,1)S(1)} %bitcast.73, bf16[768,512]{1,0:T(8,128)(2,1)S(1)} %copy-done.6), kind=kOutput, calls=%fused_computation.8 | convolution fusion | flops 1610612736 | bytes 8126464 | tf_op jit(solution)/shard_map/dot_general | solution.py:28
  249.4 4.1 %convolution_bitcast_fusion = f32[1,512,2048]{2,1,0:T(8,128)} fusion(bf16[768,2048]{1,0:T(8,128)(2,1)S(1)} %bitcast.75, f32[768,512]{1,0:T(8,128)S(1)} %copy-done.20, f32[768,512]{1,0:T(8,128)S(1)} %copy-done.21), kind=kOutput, calls=%fused_computation.6 | convolution fusion | flops 1614544896 | bytes 10485760 | tf_op jit(solution)/shard_map/dot_general | solution.py:28
  255.0 52.5 %reduce-scatter.2.cloned.1.call-done = f32[256,256]{1,0:T(8,128)} async-done(((f32[2048,256]{1,0:T(8,128)}), f32[256,256]{1,0:T(8,128)}) %reduce-scatter.2.cloned.1.call-update) | async-done | bytes 262160 | tf_op jit(solution)/shard_map/reduce_scatter | solution.py:146
  (88 shorter events, 22.6 us)
Async XLA Ops:
  7.2 92.0 %copy-start = (bf16[1,2048,512]{2,1,0:T(8,128)(2,1)S(1)}, bf16[1,2048,512]{2,1,0:T(8,128)(2,1)}, u32[]{:S(2)}) copy-start(bf16[1,2048,512]{2,1,0:T(8,128)(2,1)} %param.21) | copy-start | bytes 6291460
  7.2 86.3 %all-gather.3.cloned.1.call-start = ((), (), s32[]{:S(2)}) async-start(), calls=%async_computation.5 | async-start | bytes 3932160 | tf_op jit(solution)/shard_map/all_gather | solution.py:110
  19.1 28.7 %copy-start.3 = (bf16[192,2048]{1,0:T(8,128)(2,1)S(1)}, bf16[192,2048]{1,0:T(8,128)(2,1)}, u32[]{:S(2)}) copy-start(bf16[192,2048]{1,0:T(8,128)(2,1)} %param.13) | copy-start | bytes 2359300
  47.7 73.6 %all-gather.5.cloned.1.call-start = ((), (), s32[]{:S(2)}) async-start(), calls=%async_computation.6 | async-start | bytes 3932160 | tf_op jit(solution)/shard_map/all_gather | solution.py:111
  51.0 5.4 %copy-start.16 = (f32[192,2]{0,1:T(2,128)S(1)}, f32[192,2]{0,1:T(2,128)}, u32[]{:S(2)}) copy-start(f32[192,2]{0,1:T(2,128)} %param.15) | copy-start | bytes 4612
  93.5 5.6 %copy-start.17 = (bf16[8,96,2048]{2,1,0:T(8,128)(2,1)S(1)}, bf16[8,96,2048]{2,1,0:T(8,128)(2,1)}, u32[]{:S(2)}) copy-start(bf16[8,96,2048]{2,1,0:T(8,128)(2,1)} %all-gather.3.cloned.1.call-done) | copy-start | bytes 9437188
  127.4 2.2 copy-start.2
  172.8 5.7 %copy-start.12 = (bf16[192,256]{1,0:T(8,128)(2,1)S(1)}, bf16[192,256]{1,0:T(8,128)(2,1)}, u32[]{:S(2)}) copy-start(bf16[192,256]{1,0:T(8,128)(2,1)} %param.18) | copy-start | bytes 294916
  172.8 5.7 %copy-start.14 = (bf16[192,256]{1,0:T(8,128)(2,1)S(1)}, bf16[192,256]{1,0:T(8,128)(2,1)}, u32[]{:S(2)}) copy-start(bf16[192,256]{1,0:T(8,128)(2,1)} %param.17) | copy-start | bytes 294916
  172.8 42.3 %all-to-all-start.3 = ((f32[8,96,512]{2,1,0:T(8,128)}), f32[8,96,512]{2,1,0:T(8,128)S(1)}, u32[]{:S(2)}, u32[]{:S(2)}) async-start(f32[8,96,512]{2,1,0:T(8,128)} %bitcast.57), calls=%async_computation.3 | async-start | bytes 3145728 | tf_op jit(solution)/shard_map/all_to_all | solution.py:123
  178.4 129.1 %reduce-scatter.2.cloned.1.call-start = ((), (), s32[]{:S(2)}) async-start(), calls=%async_computation.7 | async-start | bytes 2359296 | tf_op jit(solution)/shard_map/reduce_scatter | solution.py:146
  216.7 11.0 %copy-start.11 = (bf16[192,256]{1,0:T(8,128)(2,1)S(1)}, bf16[192,256]{1,0:T(8,128)(2,1)}, u32[]{:S(2)}) copy-start(bf16[192,256]{1,0:T(8,128)(2,1)} %param.16) | copy-start | bytes 294916
  217.2 10.5 %copy-start.4 = (bf16[2048,256]{1,0:T(8,128)(2,1)S(1)}, bf16[2048,256]{1,0:T(8,128)(2,1)}, u32[]{:S(2)}) copy-start(bf16[2048,256]{1,0:T(8,128)(2,1)} %param.20) | copy-start | bytes 3145732
  228.8 5.8 %collective-permute-start = (f32[1,512]{1,0:T(1,128)S(1)}, f32[1,512]{1,0:T(1,128)S(1)}, u32[]{:S(2)}, u32[]{:S(2)}) collective-permute-start(f32[1,512]{1,0:T(1,128)S(1)} %get-tuple-element.12), channel_id=1, source_target_pairs={{0,4},{4,8},{8,12},{12,16},{16,20},{20,24},{24,28},{1,5},{5,9},{9,... | collective-permute-start | bytes 6152 | tf_op jit(solution)/shard_map/ppermute | solution.py:18
  232.1 5.5 %collective-permute-start.1 = (f32[1,512]{1,0:T(1,128)S(1)}, f32[1,512]{1,0:T(1,128)S(1)}, u32[]{:S(2)}, u32[]{:S(2)}) collective-permute-start(f32[1,512]{1,0:T(1,128)S(1)} %get-tuple-element.13), channel_id=1, source_target_pairs={{4,0},{8,4},{12,8},{16,12},{20,16},{24,20},{28,24},{5,1},{9,5},{13... | collective-permute-start | bytes 6152 | tf_op jit(solution)/shard_map/ppermute | solution.py:20
  239.5 5.9 %copy-start.6 = (bf16[768,512]{1,0:T(8,128)(2,1)S(1)}, bf16[768,512]{1,0:T(8,128)(2,1)}, u32[]{:S(2)}) copy-start(bf16[768,512]{1,0:T(8,128)(2,1)} %copy-done.5) | copy-start | bytes 2359300
  239.5 5.9 %copy-start.18 = (bf16[8,96,2048]{2,1,0:T(8,128)(2,1)S(1)}, bf16[8,96,2048]{2,1,0:T(8,128)(2,1)}, u32[]{:S(2)}) copy-start(bf16[8,96,2048]{2,1,0:T(8,128)(2,1)} %all-gather.3.cloned.1.call-done) | copy-start | bytes 9437188
  245.4 3.9 %copy-start.19 = (bf16[8,96,2048]{2,1,0:T(8,128)(2,1)S(1)}, bf16[8,96,2048]{2,1,0:T(8,128)(2,1)}, u32[]{:S(2)}) copy-start(bf16[8,96,2048]{2,1,0:T(8,128)(2,1)} %all-gather.5.cloned.1.call-done) | copy-start | bytes 9437188
  245.4 3.9 %copy-start.20 = (f32[768,512]{1,0:T(8,128)S(1)}, f32[768,512]{1,0:T(8,128)}, u32[]{:S(2)}) copy-start(f32[768,512]{1,0:T(8,128)} %fusion.1) | copy-start | bytes 4718596
  245.4 3.9 %copy-start.21 = (f32[768,512]{1,0:T(8,128)S(1)}, f32[768,512]{1,0:T(8,128)}, u32[]{:S(2)}) copy-start(f32[768,512]{1,0:T(8,128)} %fusion.7) | copy-start | bytes 4718596
  249.4 4.1 %copy-start.13 = (bf16[192,256]{1,0:T(8,128)(2,1)S(1)}, bf16[192,256]{1,0:T(8,128)(2,1)}, u32[]{:S(2)}) copy-start(bf16[192,256]{1,0:T(8,128)(2,1)} %param.18) | copy-start | bytes 294916
  249.4 4.8 %copy-start.9 = (f32[192,256]{1,0:T(8,128)S(1)}, f32[192,256]{1,0:T(8,128)}, u32[]{:S(2)}) copy-start(f32[192,256]{1,0:T(8,128)} %get-tuple-element.20) | copy-start | bytes 589828
  249.4 4.8 %copy-start.15 = (bf16[192,256]{1,0:T(8,128)(2,1)S(1)}, bf16[192,256]{1,0:T(8,128)(2,1)}, u32[]{:S(2)}) copy-start(bf16[192,256]{1,0:T(8,128)(2,1)} %param.17) | copy-start | bytes 294916
  249.4 58.1 %copy-start.1 = (bf16[1,2048,512]{2,1,0:T(8,128)(2,1)S(1)}, bf16[1,2048,512]{2,1,0:T(8,128)(2,1)}, u32[]{:S(2)}) copy-start(bf16[1,2048,512]{2,1,0:T(8,128)(2,1)} %param.21) | copy-start | bytes 6291460
  (4 other events, 6.3 us)
Sparse Core Ops, SparseCore 0:
  47.8 27.5 all-gather.2
  93.6 27.6 all-gather.4
  239.6 67.8 reduce-scatter.1
where the time goes:
time: 315 us; the launch traced here: 314 us
  waiting for transfers between devices  111 us (35%)
  blocking collectives  98.1 us (31%)
  local copies, waits for them, and re-layouts  35.8 us (11%)
  matrix products  35.3 us (11%)
  between operations  14.1 us (4%)
  starting transfers between devices  10.6 us (3%)
  other arithmetic  8.97 us (3%)
    reduce_scatter x1, waiting for transfers between devices, local(): lax.psum_scatter(contract_rows(residual, mixed_act), 'sp', scatter_dimens...  52.5 us
    all_to_all x1, blocking collectives, local(): lax.all_to_all(grouped, 'tp', split_axis=1, concat_axis=1, tiled=True)  39.4 us
    all_to_all x1, waiting for transfers between devices, local(): lax.all_to_all(shares, 'sp', split_axis=0, concat_axis=0, tiled=True)  36.5 us
    all_to_all x1, blocking collectives, local(): lax.all_to_all(sliced[0], 'sp', split_axis=0, concat_axis=0, tiled=True)  27.3 us
    all_to_all x1, blocking collectives, local(): lax.all_to_all(sliced[1], 'sp', split_axis=0, concat_axis=0, tiled=True)  23.4 us
    all_gather x1, waiting for transfers between devices, local(): lax.all_gather(arrived[1], 'tp', axis=2, tiled=True)  19.1 us
    dot_general x4, matrix products, contract_rows(): lax.dot_general(left, right, (((0,), (0,)), ((), ())), preferred_element_...  15.8 us
    dot_general x3, matrix products, contract_cols(): lax.dot_general(left, right, (((1,), (1,)), ((), ())), preferred_element_...  9.8 us
  transfers between devices with their start and end apart: 6, of which 4 were waited for; matrix products, arithmetic and copies ran while one was open for 15% of the time, Pallas kernels for 0%

commit v1 on v0

v1 whole, which is shorter than its diff:
```python
import jax
import jax.numpy as jnp
from jax import lax
from jax.sharding import PartitionSpec as P

CLAMP_LIMIT = 7.0
SILU_ALPHA = 1.702


def contract_rows(left, right):
    return lax.dot_general(
        left, right, (((0,), (0,)), ((), ())), preferred_element_type=jnp.float32
    )


def contract_cols(left, right):
    return lax.dot_general(
        left, right, (((1,), (1,)), ((), ())), preferred_element_type=jnp.float32
    )


def halo(cells, axis):
    count = lax.axis_size(axis)
    ends = count - 1
    above = lax.ppermute(cells[-1:], axis, [(i, (i + 1) % count) for i in range(ends)])
    below = lax.ppermute(cells[:1], axis, [((i + 1) % count, i) for i in range(ends)])
    return jnp.concatenate([above, cells, below], axis=0)


def exchange_groups(partial_value, part_width):
    tp_count = lax.axis_size("tp")
    pairs = tp_count // 2
    me = lax.axis_index("tp")
    side, pair = me % 2, me // 2

    def block(which_pair, which_side):
        return lax.dynamic_slice_in_dim(
            partial_value, (2 * which_pair + which_side) * part_width, part_width, 1
        )

    others = [(i, i ^ 1) for i in range(tp_count)]
    sums = []
    for step in range(1, pairs + 1):
        target = (pair + step) % pairs
        given = block(target, 1 - side).astype(jnp.bfloat16)
        got = lax.ppermute(given, "tp", others)
        sums.append(block(target, side) + got.astype(jnp.float32))
    total = sums[-1]
    for step in range(1, pairs):
        moves = [(i, (i + 2 * step) % tp_count) for i in range(tp_count)]
        got = lax.ppermute(sums[step - 1].astype(jnp.bfloat16), "tp", moves)
        total = total + got.astype(jnp.float32)
    return total


def local(
    saved_tokens,
    cotangent,
    routes,
    route_weights,
    gate_in,
    conv_in,
    value_in,
    conv_taps,
    out_weight,
    gate_proj,
    up_proj,
    down_proj,
):
    tok_rows, model_width = saved_tokens.shape
    top_count = routes.shape[1]
    expert_count = lax.axis_size("sp")
    tp_count = lax.axis_size("tp")
    capacity = 2 * tok_rows * top_count // expert_count
    slots = expert_count * capacity
    part_width = model_width // tp_count
    channels = gate_in.shape[1]
    me_tp = lax.axis_index("tp")
    offset = me_tp * part_width

    routes_t = routes.T
    weights_t = route_weights.T
    experts = lax.broadcasted_iota(jnp.int32, (expert_count, tok_rows), 0)
    chosen = [experts == routes_t[k][None, :] for k in range(top_count)]
    hits = sum(c.astype(jnp.bfloat16) for c in chosen)
    earlier = (
        lax.broadcasted_iota(jnp.int32, (tok_rows, tok_rows), 0)
        < lax.broadcasted_iota(jnp.int32, (tok_rows, tok_rows), 1)
    ).astype(jnp.bfloat16)
    before = jnp.dot(hits, earlier, preferred_element_type=jnp.float32)
    slot_ids = lax.broadcasted_iota(jnp.int32, (slots, tok_rows), 0)
    place = jnp.zeros((slots, tok_rows), jnp.float32)
    weighted = jnp.zeros((slots, tok_rows), jnp.float32)
    for k in range(top_count):
        rank = jnp.sum(jnp.where(chosen[k], before, 0.0), axis=0).astype(jnp.int32)
        here = slot_ids == (routes_t[k] * capacity + rank)[None, :]
        place = jnp.where(here, 1.0, place)
        weighted = jnp.where(here, weights_t[k][None, :], weighted)
    place = place.astype(jnp.bfloat16)
    slot_weight = jnp.sum(weighted, axis=1, keepdims=True)

    own_tokens = lax.dynamic_slice_in_dim(saved_tokens, offset, part_width, 1)
    own_cot = lax.dynamic_slice_in_dim(cotangent, offset, part_width, 1)
    send_tokens = jnp.dot(place, own_tokens, preferred_element_type=jnp.float32).astype(jnp.bfloat16)
    cot_rows = jnp.dot(place, own_cot, preferred_element_type=jnp.float32)
    send_grads = (cot_rows * slot_weight).astype(jnp.bfloat16)

    def dispatched(rows):
        rows = rows.reshape(expert_count, capacity, part_width)
        return lax.all_to_all(rows, "sp", split_axis=0, concat_axis=0, tiled=True)

    arrived_tokens = dispatched(send_tokens)
    arrived_tokens, send_grads = lax.optimization_barrier((arrived_tokens, send_grads))
    arrived_grads = dispatched(send_grads)
    rows_in = lax.all_gather(arrived_tokens, "tp", axis=2, tiled=True).reshape(slots, model_width)
    grads_in = lax.all_gather(arrived_grads, "tp", axis=2, tiled=True).reshape(slots, model_width)

    gate_f32 = gate_in.astype(jnp.float32)
    conv_f32 = conv_in.astype(jnp.float32)
    value_f32 = value_in.astype(jnp.float32)
    my_taps = lax.dynamic_slice_in_dim(conv_taps, me_tp * channels, channels, 1)
    prod_rim = halo(conv_f32 * value_f32, "sp")
    conv_out = my_taps[0] * prod_rim[:-2] + my_taps[1] * prod_rim[1:-1] + my_taps[2] * prod_rim[2:]
    mixed = gate_f32 * conv_out

    w_gate, w_up, w_down = gate_proj[0], up_proj[0], down_proj[0]
    gate_pre = jnp.dot(rows_in, w_gate, preferred_element_type=jnp.float32)
    up_pre = jnp.dot(rows_in, w_up, preferred_element_type=jnp.float32)
    gate_clip = jnp.minimum(gate_pre, CLAMP_LIMIT)
    up_clip = jnp.clip(up_pre, -CLAMP_LIMIT, CLAMP_LIMIT)
    sigmoid_gate = jax.nn.sigmoid(SILU_ALPHA * gate_clip)
    gated_act = gate_clip * sigmoid_gate
    hidden = ((up_clip + 1.0) * gated_act).astype(jnp.bfloat16)
    grads_in, mixed = lax.optimization_barrier((grads_in, mixed))
    mixed_all = lax.all_gather(mixed, "sp", axis=0, tiled=True)
    d_hidden = contract_cols(grads_in, w_down)
    d_up = jnp.where(jnp.abs(up_pre) < CLAMP_LIMIT, d_hidden * gated_act, 0.0).astype(jnp.bfloat16)
    gate_slope = sigmoid_gate + SILU_ALPHA * gate_clip * sigmoid_gate * (1.0 - sigmoid_gate)
    d_gate = jnp.where(gate_pre < CLAMP_LIMIT, d_hidden * (up_clip + 1.0) * gate_slope, 0.0).astype(
        jnp.bfloat16
    )
    partial_value = contract_cols(d_gate, w_gate) + contract_cols(d_up, w_up)
    shares = exchange_groups(partial_value, part_width).astype(jnp.bfloat16)
    down_grad = contract_rows(hidden, grads_in)
    gate_grad = contract_rows(rows_in, d_gate)
    up_grad = contract_rows(rows_in, d_up)

    returned = dispatched(shares).reshape(slots, part_width)
    combined = contract_rows(place, returned)
    token_grad = (own_cot.astype(jnp.float32) + combined).astype(jnp.bfloat16)
    residual = lax.all_gather(token_grad, "tp", axis=1, tiled=True)

    d_conv_out = jnp.dot(residual, out_weight, preferred_element_type=jnp.float32)
    grad_rim = halo(d_conv_out * gate_f32, "sp")
    d_product = my_taps[0] * grad_rim[2:] + my_taps[1] * grad_rim[1:-1] + my_taps[2] * grad_rim[:-2]
    gate_in_grad = (d_conv_out * conv_out).astype(jnp.bfloat16)
    conv_in_grad = (d_product * value_f32).astype(jnp.bfloat16)
    value_in_grad = (d_product * conv_f32).astype(jnp.bfloat16)

    share = tok_rows // tp_count
    quarter = lax.dynamic_slice_in_dim(residual, me_tp * share, share, 0)
    quarter = quarter.reshape(share, expert_count, model_width // expert_count)
    quarter = lax.all_to_all(
        quarter.transpose(1, 0, 2), "sp", split_axis=0, concat_axis=0, tiled=True
    )
    features = lax.all_gather(quarter, "tp", axis=1, tiled=True)
    features = features.reshape(expert_count * tok_rows, -1)
    mixed_all = lax.optimization_barrier(mixed_all).astype(jnp.bfloat16)
    out_weight_grad = contract_rows(features, mixed_all)
    return (
        gate_grad[None],
        up_grad[None],
        down_grad[None],
        out_weight_grad,
        token_grad,
        gate_in_grad,
        conv_in_grad,
        value_in_grad,
    )


def solution(mesh):
    in_specs = (
        P("sp", None),
        P("sp", None),
        P("sp", None),
        P("sp", None),
        P("sp", "tp"),
        P("sp", "tp"),
        P("sp", "tp"),
        P(),
        P(None, "tp"),
        P("sp", None, "tp"),
        P("sp", None, "tp"),
        P("sp", "tp", None),
    )
    out_specs = (
        P("sp", None, "tp"),
        P("sp", None, "tp"),
        P("sp", "tp", None),
        P("sp", "tp"),
        P("sp", "tp"),
        P("sp", "tp"),
        P("sp", "tp"),
        P("sp", "tp"),
    )
    return jax.shard_map(local, mesh=mesh, in_specs=in_specs, out_specs=out_specs, check_vma=False)
```

time: 315 us -> 239 us (0.76)
  waiting for transfers between devices: 111 us -> 63.8 us
  local copies, waits for them, and re-layouts: 35.8 us -> 8.37 us
  blocking collectives: 98.1 us -> 74.2 us
  starting transfers between devices: 10.6 us -> 27.7 us
  matrix products: 35.3 us -> 41.3 us
    all_to_all x3 -> x1, blocking collectives: 90.2 us -> 24 us  [dispatched(): return lax.all_to_all(rows, 'sp', split_axis=0, concat_axis=0, tiled=True)]
    reduce_scatter x1 -> x0, waiting for transfers between devices: 52.5 us -> none  [local(): lax.psum_scatter(contract_rows(residual, mixed_act), 'sp', scatter_dimens...]
    all_gather x0 -> x2, blocking collectives: none -> 42.5 us  [the longest x1 34 us: local(): mixed_all = lax.all_gather(mixed, 'sp', axis=0, tiled=True)]
    ppermute x2 -> x7, waiting for transfers between devices: 3.08 us -> 25 us  [the longest x1 19.6 us: exchange_groups(): got = lax.ppermute(sums[step - 1].astype(jnp.bfloat16), 'tp', moves)]
    gather x3 -> x0, local copies, waits for them, and re-layouts: 14.6 us -> none  [the longest x1 8.71 us: local(): jnp.concatenate([scaled.reshape(assigns, model_width), zero_row], 0)]
    all_to_all x1 -> x3, waiting for transfers between devices: 36.5 us -> 23.6 us  [the longest x2 23.6 us: dispatched(): return lax.all_to_all(rows, 'sp', split_axis=0, concat_axis=0, tiled=True)]
    all_to_all x1 -> x3, starting transfers between devices: 5.63 us -> 16.3 us  [the longest x2 12.8 us: dispatched(): return lax.all_to_all(rows, 'sp', split_axis=0, concat_axis=0, tiled=True)]
    mul x5 -> x0, local copies, waits for them, and re-layouts: 9.11 us -> none  [the longest x3 8.84 us: local(): route_weights[:, :, None] * cotangent.astype(jnp.float32)[:, None, :]]
  transfers between devices with their start and end apart: 6 -> 12, of which waited for: 4 -> 6; matrix products, arithmetic and copies ran while one was open for 15% -> 13% of each run, Pallas kernels for 0% -> 0%
where the time goes in v1:
time: 239 us; the launch traced here: 238 us
  blocking collectives  74.2 us (31%)
  waiting for transfers between devices  63.8 us (27%)
  matrix products  41.3 us (17%)
  starting transfers between devices  27.7 us (12%)
  between operations  14.3 us (6%)
  local copies, waits for them, and re-layouts  8.37 us (4%)
  other arithmetic  8.37 us (4%)
    all_gather x1, blocking collectives, local(): mixed_all = lax.all_gather(mixed, 'sp', axis=0, tiled=True)  34 us
    all_to_all x1, blocking collectives, dispatched(): return lax.all_to_all(rows, 'sp', split_axis=0, concat_axis=0, tiled=True)  24 us
    all_to_all x2, waiting for transfers between devices, dispatched(): return lax.all_to_all(rows, 'sp', split_axis=0, concat_axis=0, tiled=True)  23.6 us
    ppermute x1, waiting for transfers between devices, exchange_groups(): got = lax.ppermute(sums[step - 1].astype(jnp.bfloat16), 'tp', moves)  19.6 us
    dot_general x5, matrix products, contract_rows(): lax.dot_general(left, right, (((0,), (0,)), ((), ())), preferred_element_...  16.6 us
    all_gather x1, waiting for transfers between devices, local(): lax.all_gather(arrived_grads, 'tp', axis=2, tiled=True)  15.1 us
    all_to_all x2, starting transfers between devices, dispatched(): return lax.all_to_all(rows, 'sp', split_axis=0, concat_axis=0, tiled=True)  12.8 us
    dot_general x3, matrix products, contract_cols(): lax.dot_general(left, right, (((1,), (1,)), ((), ())), preferred_element_...  9.92 us
  transfers between devices with their start and end apart: 12, of which 6 were waited for; matrix products, arithmetic and copies ran while one was open for 13% of the time, Pallas kernels for 0%

profile of v1, /device:TPU:0, one launch (start us, length us, event | category | flops | bytes accessed | tf_op | source)
XLA Modules:
  0.0 238.0 jit_solution(18059103488705829458)
XLA Ops:
  11.3 7.3 %all-to-all-start = ((bf16[8,96,512]{2,1,0:T(8,128)(2,1)}), bf16[8,96,512]{2,1,0:T(8,128)(2,1)S(1)}, u32[]{:S(2)}, u32[]{:S(2)}) async-start(bf16[8,96,512]{2,1,0:T(8,128)(2,1)} %bitcast.61), calls=%async_computation | async-start | bytes 1572864 | tf_op jit(solution)/shard_map/all_to_all | solution.py:110
  18.8 2.3 multiply_convert_fusion.1
  21.2 17.6 %all-to-all-done = bf16[8,96,512]{2,1,0:T(8,128)(2,1)S(1)} async-done(((bf16[8,96,512]{2,1,0:T(8,128)(2,1)}), bf16[8,96,512]{2,1,0:T(8,128)(2,1)S(1)}, u32[]{:S(2)}, u32[]{:S(2)}) %all-to-all-start) | async-done | bytes 786464 | tf_op jit(solution)/shard_map/all_to_all | solution.py:110
  39.7 24.0 %all_to_all.20 = bf16[8,96,512]{2,1,0:T(8,128)(2,1)} all-to-all(bf16[8,96,512]{2,1,0:T(8,128)(2,1)} %bitcast.60), channel_id=1, replica_groups=mesh['sp'=8,'tp'=4] {'sp'}, dimensions={0} | all-to-all | bytes 1572864 | tf_op jit(solution)/shard_map/all_to_all | solution.py:110
  63.8 3.4 %collective-permute-start = (f32[1,256]{1,0:T(1,128)S(1)}, f32[1,256]{1,0:T(1,128)S(1)}, u32[]{:S(2)}, u32[]{:S(2)}) collective-permute-start(f32[1,256]{1,0:T(1,128)S(1)} %get-tuple-element.28), channel_id=1, source_target_pairs={{0,4},{4,8},{8,12},{12,16},{16,20},{20,24},{24,28},{1,5},{5,9},{9,... | collective-permute-start | bytes 3080 | tf_op jit(solution)/shard_map/ppermute | solution.py:25
  69.4 3.2 %collective-permute-done.1 = f32[1,256]{1,0:T(1,128)S(1)} collective-permute-done((f32[1,256]{1,0:T(1,128)S(1)}, f32[1,256]{1,0:T(1,128)S(1)}, u32[]{:S(2)}, u32[]{:S(2)}) %collective-permute-start.1) | collective-permute-done | bytes 1056 | tf_op jit(solution)/shard_map/ppermute | solution.py:26
  73.4 6.0 %fusion.1 = f32[768,512]{1,0:T(8,128)} fusion(bf16[768,2048]{1,0:T(8,128)(2,1)} %bitcast.91, bf16[1,2048,512]{2,1,0:T(8,128)(2,1)} %param.22), kind=kOutput, calls=%fused_computation.5 | convolution fusion | flops 1610612736 | bytes 6815744 | tf_op jit(solution)/shard_map/dot_general | solution.py:128
  79.4 3.0 %fusion.7 = f32[768,512]{1,0:T(8,128)} fusion(bf16[768,2048]{1,0:T(8,128)(2,1)S(1)} %bitcast.93, bf16[1,2048,512]{2,1,0:T(8,128)(2,1)S(1)} %copy-done), kind=kOutput, calls=%fused_computation.11 | convolution fusion | flops 1610612736 | bytes 6815744 | tf_op jit(solution)/shard_map/dot_general | solution.py:127
  82.3 15.1 %all-gather.5.cloned.1.call-done = bf16[8,96,2048]{2,1,0:T(8,128)(2,1)} async-done(((bf16[8,96,512]{2,1,0:T(8,128)(2,1)}), bf16[8,96,2048]{2,1,0:T(8,128)(2,1)}) %all-gather.5.cloned.1.call-update) | async-done | bytes 3145744 | tf_op jit(solution)/shard_map/all_gather | solution.py:116
  97.5 6.1 %select_convert_fusion = (bf16[768,512]{1,0:T(8,128)(2,1)S(1)}, bf16[768,512]{1,0:T(8,128)(2,1)S(1)}) fusion(f32[768,512]{1,0:T(8,128)} %fusion.1, f32[768,512]{1,0:T(8,128)} %fusion.7, bf16[768,2048]{1,0:T(8,128)(2,1)} %bitcast.95, bf16[1,512,2048]{2,1,0:T(8,128)(2,1)} %param.23), kind=kOutput, calls=%fused_computation.18 | convolution fusion | flops 1619263488 | bytes 9961472 | tf_op jit(solution)/shard_map/dot_general | solution.py:17
  107.5 2.6 %copy-done.1 = f32[768,2048]{1,0:T(8,128)} copy-done((f32[768,2048]{1,0:T(8,128)}, f32[768,2048]{1,0:T(8,128)S(1)}, u32[]{:S(2)}) %copy-start.1) | copy-done | bytes 6291480
  114.1 2.8 %add_convert_fusion.1 = bf16[768,512]{1,0:T(8,128)(2,1)} fusion(bf16[768,512]{1,0:T(8,128)(2,1)} %collective-permute-done.3, f32[768,2048]{1,0:T(8,128)} %copy-done.1, s32[]{:T(128)S(6)} %select_n.85), kind=kLoop, calls=%fused_computation.14 | loop fusion | flops 1179648 | bytes 3145732 | tf_op jit(solution)/shard_map/convert_element_type | solution.py:51
  117.2 19.6 %collective-permute-done.4 = bf16[768,512]{1,0:T(8,128)(2,1)} collective-permute-done((bf16[768,512]{1,0:T(8,128)(2,1)}, bf16[768,512]{1,0:T(8,128)(2,1)}, u32[]{:S(2)}, u32[]{:S(2)}) %collective-permute-start.4) | collective-permute-done | bytes 786464 | tf_op jit(solution)/shard_map/ppermute | solution.py:51
  136.9 3.1 %add_convert_fusion = bf16[768,512]{1,0:T(8,128)(2,1)} fusion(bf16[768,512]{1,0:T(8,128)(2,1)} %collective-permute-done.4, bf16[768,512]{1,0:T(8,128)(2,1)} %collective-permute-done.2, f32[768,2048]{1,0:T(8,128)} %copy-done.1, s32[]{:T(128)S(6)} %select_n.82), kind=kLoop, calls=%fused_computation.13 | loop fusion | flops 1966080 | bytes 3932164 | tf_op jit(solution)/shard_map/convert_element_type | solution.py:143
  140.0 5.5 %all-to-all-start.2 = ((bf16[8,96,512]{2,1,0:T(8,128)(2,1)}), bf16[8,96,512]{2,1,0:T(8,128)(2,1)}, u32[]{:S(2)}, u32[]{:S(2)}) async-start(bf16[8,96,512]{2,1,0:T(8,128)(2,1)} %bitcast.23), calls=%async_computation.2 | async-start | bytes 1572864 | tf_op jit(solution)/shard_map/all_to_all | solution.py:110
  145.5 5.9 %convolution_bitcast_fusion.1 = f32[1,2048,512]{2,1,0:T(8,128)} fusion(bf16[768,2048]{1,0:T(8,128)(2,1)} %bitcast.92, bf16[768,512]{1,0:T(8,128)(2,1)S(1)} %get-tuple-element.20), kind=kOutput, calls=%fused_computation.2 | convolution fusion | flops 1610612736 | bytes 8126464 | tf_op jit(solution)/shard_map/dot_general | solution.py:11
  151.4 3.9 %convolution_bitcast_fusion.2 = f32[1,2048,512]{2,1,0:T(8,128)} fusion(bf16[768,2048]{1,0:T(8,128)(2,1)S(1)} %bitcast.94, bf16[768,512]{1,0:T(8,128)(2,1)S(1)} %copy-done.6), kind=kOutput, calls=%fused_computation.3 | convolution fusion | flops 1610612736 | bytes 8126464 | tf_op jit(solution)/shard_map/dot_general | solution.py:11
  155.3 4.1 %convolution_bitcast_fusion = f32[1,512,2048]{2,1,0:T(8,128)} fusion(bf16[768,2048]{1,0:T(8,128)(2,1)S(1)} %bitcast.96, f32[768,512]{1,0:T(8,128)S(1)} %copy-done.15, f32[768,512]{1,0:T(8,128)S(1)} %copy-done.16), kind=kOutput, calls=%fused_computation.1 | convolution fusion | flops 1614544896 | bytes 10485760 | tf_op jit(solution)/shard_map/dot_general | solution.py:11
  159.4 6.0 %all-to-all-done.2 = bf16[8,96,512]{2,1,0:T(8,128)(2,1)} async-done(((bf16[8,96,512]{2,1,0:T(8,128)(2,1)}), bf16[8,96,512]{2,1,0:T(8,128)(2,1)}, u32[]{:S(2)}, u32[]{:S(2)}) %all-to-all-start.2) | async-done | bytes 786464 | tf_op jit(solution)/shard_map/all_to_all | solution.py:110
  167.7 7.6 %all_gather.17 = bf16[192,2048]{1,0:T(8,128)(2,1)S(1)} all-gather(bf16[192,512]{1,0:T(8,128)(2,1)S(1)} %fusion.9), channel_id=1, replica_groups=mesh['sp'=8,'tp'=4] {'tp'}, dimensions={1}, use_global_device_ids=true | all-gather | bytes 983040 | tf_op jit(solution)/shard_map/all_gather | solution.py:151
  177.7 4.5 %collective-permute-start.6 = (f32[1,256]{1,0:T(1,128)S(1)}, f32[1,256]{1,0:T(1,128)S(1)}, u32[]{:S(2)}, u32[]{:S(2)}) collective-permute-start(f32[1,256]{1,0:T(1,128)S(1)} %get-tuple-element.25), channel_id=1, source_target_pairs={{0,4},{4,8},{8,12},{12,16},{16,20},{20,24},{24,28},{1,5},{5,9},{9,... | collective-permute-start | bytes 3080 | tf_op jit(solution)/shard_map/ppermute | solution.py:25
  183.0 3.5 %all-to-all-start.3 = ((bf16[8,48,256]{2,1,0:T(8,128)(2,1)}), bf16[8,48,256]{2,1,0:T(8,128)(2,1)S(1)}, u32[]{:S(2)}, u32[]{:S(2)}) async-start(bf16[8,48,256]{2,1,0:T(8,128)(2,1)} %copy.24), calls=%async_computation.3 | async-start | bytes 393216 | tf_op jit(solution)/shard_map/all_to_all | solution.py:163
  186.5 34.0 %all_gather.19 = bf16[1536,256]{1,0:T(8,128)(2,1)S(1)} all-gather(bf16[192,256]{1,0:T(8,128)(2,1)} %convert_multiply_fusion.4), channel_id=1, replica_groups=mesh['sp'=8,'tp'=4] {'sp'}, dimensions={0}, use_global_device_ids=true | all-gather | bytes 884736 | tf_op jit(solution)/shard_map/all_gather | solution.py:135
  221.3 8.6 %all_gather.18 = bf16[8,192,256]{2,0,1:T(8,128)(2,1)S(1)} all-gather(bf16[8,48,256]{2,0,1:T(8,128)(2,1)S(1)} %copy.25), channel_id=1, replica_groups=mesh['sp'=8,'tp'=4] {'tp'}, dimensions={1}, use_global_device_ids=true | all-gather | bytes 983040 | tf_op jit(solution)/shard_map/all_gather | solution.py:166
  (74 shorter events, 23.9 us)
Async XLA Ops:
  7.2 72.2 %copy-start = (bf16[1,2048,512]{2,1,0:T(8,128)(2,1)S(1)}, bf16[1,2048,512]{2,1,0:T(8,128)(2,1)}, u32[]{:S(2)}) copy-start(bf16[1,2048,512]{2,1,0:T(8,128)(2,1)} %param.21) | copy-start | bytes 6291460
  9.0 9.7 %copy-start.11 = (f32[192,2]{0,1:T(2,128)S(1)}, f32[192,2]{0,1:T(2,128)}, u32[]{:S(2)}) copy-start(f32[192,2]{0,1:T(2,128)} %param.15) | copy-start | bytes 4612
  11.3 27.5 %all-to-all-start = ((bf16[8,96,512]{2,1,0:T(8,128)(2,1)}), bf16[8,96,512]{2,1,0:T(8,128)(2,1)S(1)}, u32[]{:S(2)}, u32[]{:S(2)}) async-start(bf16[8,96,512]{2,1,0:T(8,128)(2,1)} %bitcast.61), calls=%async_computation | async-start | bytes 1572864 | tf_op jit(solution)/shard_map/all_to_all | solution.py:110
  18.6 54.8 %all-gather.3.cloned.1.call-start = ((), (), s32[]{:S(2)}) async-start(), calls=%async_computation.4 | async-start | bytes 3932160 | tf_op jit(solution)/shard_map/all_gather | solution.py:115
  38.8 25.0 %copy-start.8 = (bf16[192,256]{1,0:T(8,128)(2,1)S(1)}, bf16[192,256]{1,0:T(8,128)(2,1)}, u32[]{:S(2)}) copy-start(bf16[192,256]{1,0:T(8,128)(2,1)} %param.18) | copy-start | bytes 294916
  38.8 25.0 %copy-start.9 = (bf16[192,256]{1,0:T(8,128)(2,1)S(1)}, bf16[192,256]{1,0:T(8,128)(2,1)}, u32[]{:S(2)}) copy-start(bf16[192,256]{1,0:T(8,128)(2,1)} %param.17) | copy-start | bytes 294916
  39.7 33.0 %copy-start.7 = (bf16[192,256]{1,0:T(8,128)(2,1)S(1)}, bf16[192,256]{1,0:T(8,128)(2,1)}, u32[]{:S(2)}) copy-start(bf16[192,256]{1,0:T(8,128)(2,1)} %param.16) | copy-start | bytes 294916
  39.7 57.8 %all-gather.5.cloned.1.call-start = ((), (), s32[]{:S(2)}) async-start(), calls=%async_computation.5 | async-start | bytes 3932160 | tf_op jit(solution)/shard_map/all_gather | solution.py:116
  63.8 5.6 %collective-permute-start = (f32[1,256]{1,0:T(1,128)S(1)}, f32[1,256]{1,0:T(1,128)S(1)}, u32[]{:S(2)}, u32[]{:S(2)}) collective-permute-start(f32[1,256]{1,0:T(1,128)S(1)} %get-tuple-element.28), channel_id=1, source_target_pairs={{0,4},{4,8},{8,12},{12,16},{16,20},{20,24},{24,28},{1,5},{5,9},{9,... | collective-permute-start | bytes 3080 | tf_op jit(solution)/shard_map/ppermute | solution.py:25
  67.2 5.5 %collective-permute-start.1 = (f32[1,256]{1,0:T(1,128)S(1)}, f32[1,256]{1,0:T(1,128)S(1)}, u32[]{:S(2)}, u32[]{:S(2)}) collective-permute-start(f32[1,256]{1,0:T(1,128)S(1)} %get-tuple-element.29), channel_id=1, source_target_pairs={{4,0},{8,4},{12,8},{16,12},{20,16},{24,20},{28,24},{5,1},{9,5},{13... | collective-permute-start | bytes 3080 | tf_op jit(solution)/shard_map/ppermute | solution.py:26
  73.4 6.0 %copy-start.12 = (bf16[8,96,2048]{2,1,0:T(8,128)(2,1)S(1)}, bf16[8,96,2048]{2,1,0:T(8,128)(2,1)}, u32[]{:S(2)}) copy-start(bf16[8,96,2048]{2,1,0:T(8,128)(2,1)} %all-gather.3.cloned.1.call-done) | copy-start | bytes 9437188
  111.5 2.6 %collective-permute-start.3 = (bf16[768,512]{1,0:T(8,128)(2,1)}, bf16[768,512]{1,0:T(8,128)(2,1)}, u32[]{:S(2)}, u32[]{:S(2)}) collective-permute-start(bf16[768,512]{1,0:T(8,128)(2,1)} %get-tuple-element.19), channel_id=1, source_target_pairs={{0,1},{1,0},{2,3},{3,2},{4,5},{5,4},{6,7},{7,6},{8,9},{9,8},{10,11... | collective-permute-start | bytes 2359304 | tf_op jit(solution)/shard_map/ppermute | solution.py:46
  111.7 5.5 %collective-permute-start.2 = (bf16[768,512]{1,0:T(8,128)(2,1)}, bf16[768,512]{1,0:T(8,128)(2,1)}, u32[]{:S(2)}, u32[]{:S(2)}) collective-permute-start(bf16[768,512]{1,0:T(8,128)(2,1)} %get-tuple-element.18), channel_id=1, source_target_pairs={{0,1},{1,0},{2,3},{3,2},{4,5},{5,4},{6,7},{7,6},{8,9},{9,8},{10,11... | collective-permute-start | bytes 2359304 | tf_op jit(solution)/shard_map/ppermute | solution.py:46
  116.9 20.0 %collective-permute-start.4 = (bf16[768,512]{1,0:T(8,128)(2,1)}, bf16[768,512]{1,0:T(8,128)(2,1)}, u32[]{:S(2)}, u32[]{:S(2)}) collective-permute-start(bf16[768,512]{1,0:T(8,128)(2,1)} %add_convert_fusion.1), channel_id=1, source_target_pairs={{0,2},{1,3},{2,0},{3,1},{4,6},{5,7},{6,4},{7,5},{8,10},{9,11},{10,... | collective-permute-start | bytes 2359304 | tf_op jit(solution)/shard_map/ppermute | solution.py:51
  140.0 25.4 %all-to-all-start.2 = ((bf16[8,96,512]{2,1,0:T(8,128)(2,1)}), bf16[8,96,512]{2,1,0:T(8,128)(2,1)}, u32[]{:S(2)}, u32[]{:S(2)}) async-start(bf16[8,96,512]{2,1,0:T(8,128)(2,1)} %bitcast.23), calls=%async_computation.2 | async-start | bytes 1572864 | tf_op jit(solution)/shard_map/all_to_all | solution.py:110
  145.5 5.9 %copy-start.6 = (bf16[768,512]{1,0:T(8,128)(2,1)S(1)}, bf16[768,512]{1,0:T(8,128)(2,1)}, u32[]{:S(2)}) copy-start(bf16[768,512]{1,0:T(8,128)(2,1)} %copy-done.5) | copy-start | bytes 2359300
  145.5 5.9 %copy-start.13 = (bf16[8,96,2048]{2,1,0:T(8,128)(2,1)S(1)}, bf16[8,96,2048]{2,1,0:T(8,128)(2,1)}, u32[]{:S(2)}) copy-start(bf16[8,96,2048]{2,1,0:T(8,128)(2,1)} %all-gather.3.cloned.1.call-done) | copy-start | bytes 9437188
  151.4 3.9 %copy-start.14 = (bf16[8,96,2048]{2,1,0:T(8,128)(2,1)S(1)}, bf16[8,96,2048]{2,1,0:T(8,128)(2,1)}, u32[]{:S(2)}) copy-start(bf16[8,96,2048]{2,1,0:T(8,128)(2,1)} %all-gather.5.cloned.1.call-done) | copy-start | bytes 9437188
  151.4 3.9 %copy-start.15 = (f32[768,512]{1,0:T(8,128)S(1)}, f32[768,512]{1,0:T(8,128)}, u32[]{:S(2)}) copy-start(f32[768,512]{1,0:T(8,128)} %fusion.1) | copy-start | bytes 4718596
  151.4 3.9 %copy-start.16 = (f32[768,512]{1,0:T(8,128)S(1)}, f32[768,512]{1,0:T(8,128)}, u32[]{:S(2)}) copy-start(f32[768,512]{1,0:T(8,128)} %fusion.7) | copy-start | bytes 4718596
  165.4 10.0 %copy-start.4 = (bf16[2048,256]{1,0:T(8,128)(2,1)S(1)}, bf16[2048,256]{1,0:T(8,128)(2,1)}, u32[]{:S(2)}) copy-start(bf16[2048,256]{1,0:T(8,128)(2,1)} %param.20) | copy-start | bytes 3145732
  176.4 44.1 %collective-permute-start.5 = (f32[1,256]{1,0:T(1,128)S(1)}, f32[1,256]{1,0:T(1,128)S(1)}, u32[]{:S(2)}, u32[]{:S(2)}) collective-permute-start(f32[1,256]{1,0:T(1,128)S(1)} %get-tuple-element.24), channel_id=1, source_target_pairs={{4,0},{8,4},{12,8},{16,12},{20,16},{24,20},{28,24},{5,1},{9,5},{13... | collective-permute-start | bytes 3080 | tf_op jit(solution)/shard_map/ppermute | solution.py:26
  177.7 42.8 %collective-permute-start.6 = (f32[1,256]{1,0:T(1,128)S(1)}, f32[1,256]{1,0:T(1,128)S(1)}, u32[]{:S(2)}, u32[]{:S(2)}) collective-permute-start(f32[1,256]{1,0:T(1,128)S(1)} %get-tuple-element.25), channel_id=1, source_target_pairs={{0,4},{4,8},{8,12},{12,16},{16,20},{20,24},{24,28},{1,5},{5,9},{9,... | collective-permute-start | bytes 3080 | tf_op jit(solution)/shard_map/ppermute | solution.py:25
  183.0 38.3 %all-to-all-start.3 = ((bf16[8,48,256]{2,1,0:T(8,128)(2,1)}), bf16[8,48,256]{2,1,0:T(8,128)(2,1)S(1)}, u32[]{:S(2)}, u32[]{:S(2)}) async-start(bf16[8,48,256]{2,1,0:T(8,128)(2,1)} %copy.24), calls=%async_computation.3 | async-start | bytes 393216 | tf_op jit(solution)/shard_map/all_to_all | solution.py:163
  (5 other events, 7.9 us)
Sparse Core Ops, SparseCore 0:
  39.8 27.5 all-gather.2
  68.9 28.5 all-gather.4

commit v2 on v1

--- a/solution.py
+++ b/solution.py
@@ -51,6 +51,26 @@
         got = lax.ppermute(sums[step - 1].astype(jnp.bfloat16), "tp", moves)
         total = total + got.astype(jnp.float32)
     return total
+
+
+def gather_features(part):
+    tp_count = lax.axis_size("tp")
+    pairs = tp_count // 2
+    me = lax.axis_index("tp")
+    side, pair = me % 2, me // 2
+    width = part.shape[1]
+    others = [(i, i ^ 1) for i in range(tp_count)]
+    held = [part]
+    for step in range(1, pairs):
+        moves = [(i, (i + 2 * step) % tp_count) for i in range(tp_count)]
+        held.append(lax.ppermute(part, "tp", moves))
+    twins = [lax.ppermute(block, "tp", others) for block in held]
+    whole = jnp.zeros((part.shape[0], tp_count * width), part.dtype)
+    for step in range(pairs):
+        first = 2 * ((pair - step) % pairs)
+        whole = lax.dynamic_update_slice_in_dim(whole, held[step], (first + side) * width, 1)
+        whole = lax.dynamic_update_slice_in_dim(whole, twins[step], (first + 1 - side) * width, 1)
+    return whole
 
 
 def local(
@@ -112,8 +132,8 @@
     arrived_tokens = dispatched(send_tokens)
     arrived_tokens, send_grads = lax.optimization_barrier((arrived_tokens, send_grads))
     arrived_grads = dispatched(send_grads)
-    rows_in = lax.all_gather(arrived_tokens, "tp", axis=2, tiled=True).reshape(slots, model_width)
-    grads_in = lax.all_gather(arrived_grads, "tp", axis=2, tiled=True).reshape(slots, model_width)
+    rows_in = gather_features(arrived_tokens.reshape(slots, part_width))
+    grads_in = gather_features(arrived_grads.reshape(slots, part_width))
 
     gate_f32 = gate_in.astype(jnp.float32)
     conv_f32 = conv_in.astype(jnp.float32)
@@ -121,7 +141,8 @@
     my_taps = lax.dynamic_slice_in_dim(conv_taps, me_tp * channels, channels, 1)
     prod_rim = halo(conv_f32 * value_f32, "sp")
     conv_out = my_taps[0] * prod_rim[:-2] + my_taps[1] * prod_rim[1:-1] + my_taps[2] * prod_rim[2:]
-    mixed = gate_f32 * conv_out
+    mixed = (gate_f32 * conv_out).astype(jnp.bfloat16)
+    mixed = jnp.concatenate([mixed, mixed], axis=1)
 
     w_gate, w_up, w_down = gate_proj[0], up_proj[0], down_proj[0]
     gate_pre = jnp.dot(rows_in, w_gate, preferred_element_type=jnp.float32)
@@ -165,8 +186,7 @@
     )
     features = lax.all_gather(quarter, "tp", axis=1, tiled=True)
     features = features.reshape(expert_count * tok_rows, -1)
-    mixed_all = lax.optimization_barrier(mixed_all).astype(jnp.bfloat16)
-    out_weight_grad = contract_rows(features, mixed_all)
+    out_weight_grad = contract_rows(features, mixed_all[:, :channels])
     return (
         gate_grad[None],
         up_grad[None],

time: 239 us -> 217 us (0.908)
  blocking collectives: 74.2 us -> 16.9 us
  starting transfers between devices: 27.7 us -> 41.2 us
  local copies, waits for them, and re-layouts: 8.37 us -> 21.8 us
  waiting for transfers between devices: 63.8 us -> 70.4 us
    all_gather x1 -> x0, blocking collectives: 34 us -> none  [local(): mixed_all = lax.all_gather(mixed, 'sp', axis=0, tiled=True)]
    all_to_all x1 -> x0, blocking collectives: 24 us -> none  [dispatched(): return lax.all_to_all(rows, 'sp', split_axis=0, concat_axis=0, tiled=True)]
    ppermute x0 -> x6, waiting for transfers between devices: none -> 18.2 us  [the longest x2 18.2 us: gather_features(): held.append(lax.ppermute(part, 'tp', moves))]
    all_gather x2 -> x1, waiting for transfers between devices: 15.1 us -> 0.01 us  [local(): mixed_all = lax.all_gather(mixed, 'sp', axis=0, tiled=True)]
    dynamic_update_slice x0 -> x8, local copies, waits for them, and re-layouts: none -> 9.13 us  [the longest x4 4.62 us: gather_features(): lax.dynamic_update_slice_in_dim(whole, twins[step], (first + 1 - side) *...]
    all_to_all x2 -> x3, starting transfers between devices: 12.8 us -> 20.5 us  [dispatched(): return lax.all_to_all(rows, 'sp', split_axis=0, concat_axis=0, tiled=True)]
    all_to_all x2 -> x3, waiting for transfers between devices: 23.6 us -> 29.6 us  [dispatched(): return lax.all_to_all(rows, 'sp', split_axis=0, concat_axis=0, tiled=True)]
    dot_general x5, matrix products: 16.6 us -> 22.6 us  [contract_rows(): lax.dot_general(left, right, (((0,), (0,)), ((), ())), preferred_element_...]
  transfers between devices with their start and end apart: 12 -> 18, of which waited for: 6 -> 7; matrix products, arithmetic and copies ran while one was open for 13% -> 23% of each run, Pallas kernels for 0% -> 0%
where the time goes in v2:
time: 217 us; the launch traced here: 216 us
  waiting for transfers between devices  70.4 us (32%)
  matrix products  42.5 us (20%)
  starting transfers between devices  41.2 us (19%)
  local copies, waits for them, and re-layouts  21.8 us (10%)
  blocking collectives  16.9 us (8%)
  between operations  14.5 us (7%)
  other arithmetic  8.44 us (4%)
    all_to_all x3, waiting for transfers between devices, dispatched(): return lax.all_to_all(rows, 'sp', split_axis=0, concat_axis=0, tiled=True)  29.6 us
    dot_general x5, matrix products, contract_rows(): lax.dot_general(left, right, (((0,), (0,)), ((), ())), preferred_element_...  22.6 us
    all_to_all x3, starting transfers between devices, dispatched(): return lax.all_to_all(rows, 'sp', split_axis=0, concat_axis=0, tiled=True)  20.5 us
    ppermute x1, waiting for transfers between devices, exchange_groups(): got = lax.ppermute(sums[step - 1].astype(jnp.bfloat16), 'tp', moves)  18.6 us
    ppermute x2, waiting for transfers between devices, gather_features(): held.append(lax.ppermute(part, 'tp', moves))  18.2 us
    all_gather x1, blocking collectives, local(): features = lax.all_gather(quarter, 'tp', axis=1, tiled=True)  8.84 us
    ppermute x2, starting transfers between devices, halo(): lax.ppermute(cells[-1:], axis, [(i, (i + 1) % count) for i in range(ends)])  8.46 us
    all_gather x1, blocking collectives, local(): residual = lax.all_gather(token_grad, 'tp', axis=1, tiled=True)  8.05 us
  transfers between devices with their start and end apart: 18, of which 7 were waited for; matrix products, arithmetic and copies ran while one was open for 23% of the time, Pallas kernels for 0%

profile of v2, /device:TPU:0, one launch (start us, length us, event | category | flops | bytes accessed | tf_op | source)
XLA Modules:
  0.0 215.5 jit_solution(15205514426126750161)
XLA Ops:
  11.3 7.3 %all-to-all-start = ((bf16[8,96,512]{2,1,0:T(8,128)(2,1)}), bf16[8,96,512]{2,1,0:T(8,128)(2,1)}, u32[]{:S(2)}, u32[]{:S(2)}) async-start(bf16[8,96,512]{2,1,0:T(8,128)(2,1)} %bitcast.7), calls=%async_computation | async-start | bytes 1572864 | tf_op jit(solution)/shard_map/all_to_all | solution.py:130
  18.8 2.4 %multiply_convert_fusion.1 = bf16[768,512]{1,0:T(8,128)(2,1)} fusion(f32[768]{0:T(1024)S(1)} %select_reduce_fusion, s32[192]{0:T(256)S(1)} %bitcast.85, s32[192]{0:T(256)S(1)} %bitcast.81, bf16[192,2048]{1,0:T(8,128)(2,1)} %param.13, s32[]{:T(128)S(6)} %select_n.107), kind=kOutput, calls=%fused_computation.23 | convolution fusion | flops 152518656 | bytes 987652 | tf_op jit(solution)/shard_map/dot_general | solution.py:125
  21.2 17.7 %all-to-all-done = bf16[8,96,512]{2,1,0:T(8,128)(2,1)} async-done(((bf16[8,96,512]{2,1,0:T(8,128)(2,1)}), bf16[8,96,512]{2,1,0:T(8,128)(2,1)}, u32[]{:S(2)}, u32[]{:S(2)}) %all-to-all-start) | async-done | bytes 786464 | tf_op jit(solution)/shard_map/all_to_all | solution.py:130
  40.4 3.6 %all-to-all-start.1 = ((bf16[8,96,512]{2,1,0:T(8,128)(2,1)}), bf16[8,96,512]{2,1,0:T(8,128)(2,1)S(1)}, u32[]{:S(2)}, u32[]{:S(2)}) async-start(bf16[8,96,512]{2,1,0:T(8,128)(2,1)} %bitcast.62), calls=%async_computation.1 | async-start | bytes 1572864 | tf_op jit(solution)/shard_map/all_to_all | solution.py:130
  44.1 3.9 %collective-permute-start.6 = (f32[1,256]{1,0:T(1,128)S(1)}, f32[1,256]{1,0:T(1,128)S(1)}, u32[]{:S(2)}, u32[]{:S(2)}) collective-permute-start(f32[1,256]{1,0:T(1,128)S(1)} %get-tuple-element.28), channel_id=1, source_target_pairs={{0,4},{4,8},{8,12},{12,16},{16,20},{20,24},{24,28},{1,5},{5,9},{9,... | collective-permute-start | bytes 3080 | tf_op jit(solution)/shard_map/ppermute | solution.py:25
  50.3 6.8 %collective-permute-done.1 = bf16[768,512]{1,0:T(8,128)(2,1)} collective-permute-done((bf16[768,512]{1,0:T(8,128)(2,1)}, bf16[768,512]{1,0:T(8,128)(2,1)}, u32[]{:S(2)}, u32[]{:S(2)}) %collective-permute-start.1) | collective-permute-done | bytes 786464 | tf_op jit(solution)/shard_map/ppermute | solution.py:66
  71.3 3.7 %fusion.1 = f32[768,512]{1,0:T(8,128)S(1)} fusion(bf16[768,2048]{1,0:T(8,128)(2,1)} %constant_dynamic-update-slice_fusion.4, bf16[1,2048,512]{2,1,0:T(8,128)(2,1)S(1)} %copy-done.3), kind=kOutput, calls=%fused_computation.5 | convolution fusion | flops 1610612736 | bytes 6815744 | tf_op jit(solution)/shard_map/dot_general | solution.py:149
  75.0 11.4 %collective-permute-done.4 = bf16[768,512]{1,0:T(8,128)(2,1)S(1)} collective-permute-done((bf16[768,512]{1,0:T(8,128)(2,1)S(1)}, bf16[768,512]{1,0:T(8,128)(2,1)S(1)}, u32[]{:S(2)}, u32[]{:S(2)}) %collective-permute-start.4) | collective-permute-done | bytes 786464 | tf_op jit(solution)/shard_map/ppermute | solution.py:66
  86.4 3.7 %fusion.7 = f32[768,512]{1,0:T(8,128)S(1)} fusion(bf16[768,2048]{1,0:T(8,128)(2,1)} %constant_dynamic-update-slice_fusion.4, bf16[1,2048,512]{2,1,0:T(8,128)(2,1)S(1)} %copy-done), kind=kOutput, calls=%fused_computation.11 | convolution fusion | flops 1610612736 | bytes 6815744 | tf_op jit(solution)/shard_map/dot_general | solution.py:148
  92.2 2.8 %select_convert_fusion = (bf16[768,512]{1,0:T(8,128)(2,1)S(1)}, bf16[768,512]{1,0:T(8,128)(2,1)S(1)}) fusion(f32[768,512]{1,0:T(8,128)S(1)} %fusion.1, f32[768,512]{1,0:T(8,128)S(1)} %fusion.7, bf16[768,2048]{1,0:T(8,128)(2,1)S(1)} %constant_dynamic-update-slice_fusion, bf16[1,512,2048]{2,1,0:T(8,128)(2,1)S(1)} %copy-done.11), kind=kOutput, calls=%fused_computation.18 | convolution fusion | flops 1619263488 | bytes 9961472 | tf_op jit(solution)/shard_map/dot_general | solution.py:17
  98.9 2.6 %copy-done.1 = f32[768,2048]{1,0:T(8,128)} copy-done((f32[768,2048]{1,0:T(8,128)}, f32[768,2048]{1,0:T(8,128)S(1)}, u32[]{:S(2)}) %copy-start.1) | copy-done | bytes 6291480
  105.7 2.8 %add_convert_fusion.1 = bf16[768,512]{1,0:T(8,128)(2,1)} fusion(bf16[768,512]{1,0:T(8,128)(2,1)} %collective-permute-done.9, f32[768,2048]{1,0:T(8,128)} %copy-done.1, s32[]{:T(128)S(6)} %select_n.125), kind=kLoop, calls=%fused_computation.14 | loop fusion | flops 1179648 | bytes 3145732 | tf_op jit(solution)/shard_map/convert_element_type | solution.py:51
  110.0 18.6 %collective-permute-done.10 = bf16[768,512]{1,0:T(8,128)(2,1)} collective-permute-done((bf16[768,512]{1,0:T(8,128)(2,1)}, bf16[768,512]{1,0:T(8,128)(2,1)}, u32[]{:S(2)}, u32[]{:S(2)}) %collective-permute-start.10) | collective-permute-done | bytes 786464 | tf_op jit(solution)/shard_map/ppermute | solution.py:51
  128.6 3.1 %add_convert_fusion = bf16[768,512]{1,0:T(8,128)(2,1)} fusion(bf16[768,512]{1,0:T(8,128)(2,1)} %collective-permute-done.10, bf16[768,512]{1,0:T(8,128)(2,1)} %collective-permute-done.8, f32[768,2048]{1,0:T(8,128)} %copy-done.1, s32[]{:T(128)S(6)} %select_n.122), kind=kLoop, calls=%fused_computation.13 | loop fusion | flops 1966080 | bytes 3932164 | tf_op jit(solution)/shard_map/convert_element_type | solution.py:164
  131.7 9.7 %all-to-all-start.2 = ((bf16[8,96,512]{2,1,0:T(8,128)(2,1)}), bf16[8,96,512]{2,1,0:T(8,128)(2,1)}, u32[]{:S(2)}, u32[]{:S(2)}) async-start(bf16[8,96,512]{2,1,0:T(8,128)(2,1)} %bitcast.23), calls=%async_computation.2 | async-start | bytes 1572864 | tf_op jit(solution)/shard_map/all_to_all | solution.py:130
  142.2 6.9 %convolution_bitcast_fusion = f32[1,512,2048]{2,1,0:T(8,128)} fusion(bf16[768,2048]{1,0:T(8,128)(2,1)} %copy-done.2, f32[768,512]{1,0:T(8,128)} %copy-done.12, f32[768,512]{1,0:T(8,128)} %copy-done.13), kind=kOutput, calls=%fused_computation.1 | convolution fusion | flops 1614544896 | bytes 10485760 | tf_op jit(solution)/shard_map/dot_general | solution.py:11
  149.0 5.7 %convolution_bitcast_fusion.1 = f32[1,2048,512]{2,1,0:T(8,128)} fusion(bf16[768,2048]{1,0:T(8,128)(2,1)} %constant_dynamic-update-slice_fusion.4, bf16[768,512]{1,0:T(8,128)(2,1)S(1)} %get-tuple-element.20), kind=kOutput, calls=%fused_computation.2 | convolution fusion | flops 1610612736 | bytes 8126464 | tf_op jit(solution)/shard_map/dot_general | solution.py:11
  154.8 11.9 %all-to-all-done.2 = bf16[8,96,512]{2,1,0:T(8,128)(2,1)} async-done(((bf16[8,96,512]{2,1,0:T(8,128)(2,1)}), bf16[8,96,512]{2,1,0:T(8,128)(2,1)}, u32[]{:S(2)}, u32[]{:S(2)}) %all-to-all-start.2) | async-done | bytes 786464 | tf_op jit(solution)/shard_map/all_to_all | solution.py:130
  169.0 8.0 %all_gather.9 = bf16[192,2048]{1,0:T(8,128)(2,1)S(1)} all-gather(bf16[192,512]{1,0:T(8,128)(2,1)S(1)} %fusion.9), channel_id=1, replica_groups=mesh['sp'=8,'tp'=4] {'tp'}, dimensions={1}, use_global_device_ids=true | all-gather | bytes 983040 | tf_op jit(solution)/shard_map/all_gather | solution.py:172
  179.4 4.5 %collective-permute-start.12 = (f32[1,256]{1,0:T(1,128)S(1)}, f32[1,256]{1,0:T(1,128)S(1)}, u32[]{:S(2)}, u32[]{:S(2)}) collective-permute-start(f32[1,256]{1,0:T(1,128)S(1)} %get-tuple-element.25), channel_id=1, source_target_pairs={{0,4},{4,8},{8,12},{12,16},{16,20},{20,24},{24,28},{1,5},{5,9},{9,... | collective-permute-start | bytes 3080 | tf_op jit(solution)/shard_map/ppermute | solution.py:25
  184.7 3.6 %all-to-all-start.3 = ((bf16[8,48,256]{2,1,0:T(8,128)(2,1)}), bf16[8,48,256]{2,1,0:T(8,128)(2,1)S(1)}, u32[]{:S(2)}, u32[]{:S(2)}) async-start(bf16[8,48,256]{2,1,0:T(8,128)(2,1)} %copy.24), calls=%async_computation.3 | async-start | bytes 393216 | tf_op jit(solution)/shard_map/all_to_all | solution.py:184
  188.4 5.9 %convolution_bitcast_fusion.2 = f32[1,2048,512]{2,1,0:T(8,128)} fusion(bf16[768,2048]{1,0:T(8,128)(2,1)} %constant_dynamic-update-slice_fusion.4, bf16[768,512]{1,0:T(8,128)(2,1)} %copy-done.5), kind=kOutput, calls=%fused_computation.3 | convolution fusion | flops 1610612736 | bytes 8126464 | tf_op jit(solution)/shard_map/dot_general | solution.py:11
  196.3 8.8 %all_gather.10 = bf16[8,192,256]{2,0,1:T(8,128)(2,1)S(1)} all-gather(bf16[8,48,256]{2,0,1:T(8,128)(2,1)S(1)} %copy.25), channel_id=1, replica_groups=mesh['sp'=8,'tp'=4] {'tp'}, dimensions={1}, use_global_device_ids=true | all-gather | bytes 983040 | tf_op jit(solution)/shard_map/all_gather | solution.py:187
  206.2 2.5 %fusion.10 = f32[256,256]{1,0:T(8,128)} fusion(bf16[1536,256]{1,0:T(8,128)(2,1)} %bitcast.63, bf16[1536,512]{1,0:T(8,128)(2,1)} %all-gather.2.cloned.1.call-done), kind=kOutput, calls=%fused_computation.28 | convolution fusion | flops 201326592 | bytes 1835008 | tf_op jit(solution)/shard_map/dot_general | solution.py:11
  (88 shorter events, 43.0 us)
Async XLA Ops:
  7.2 79.2 %copy-start = (bf16[1,2048,512]{2,1,0:T(8,128)(2,1)S(1)}, bf16[1,2048,512]{2,1,0:T(8,128)(2,1)}, u32[]{:S(2)}) copy-start(bf16[1,2048,512]{2,1,0:T(8,128)(2,1)} %param.21) | copy-start | bytes 6291460
  7.2 11.4 %copy-start.10 = (f32[192,2]{0,1:T(2,128)S(1)}, f32[192,2]{0,1:T(2,128)}, u32[]{:S(2)}) copy-start(f32[192,2]{0,1:T(2,128)} %param.15) | copy-start | bytes 4612
  11.3 27.6 %all-to-all-start = ((bf16[8,96,512]{2,1,0:T(8,128)(2,1)}), bf16[8,96,512]{2,1,0:T(8,128)(2,1)}, u32[]{:S(2)}, u32[]{:S(2)}) async-start(bf16[8,96,512]{2,1,0:T(8,128)(2,1)} %bitcast.7), calls=%async_computation | async-start | bytes 1572864 | tf_op jit(solution)/shard_map/all_to_all | solution.py:130
  18.6 25.4 %copy-start.7 = (bf16[192,256]{1,0:T(8,128)(2,1)S(1)}, bf16[192,256]{1,0:T(8,128)(2,1)}, u32[]{:S(2)}) copy-start(bf16[192,256]{1,0:T(8,128)(2,1)} %param.18) | copy-start | bytes 294916
  18.6 25.4 %copy-start.8 = (bf16[192,256]{1,0:T(8,128)(2,1)S(1)}, bf16[192,256]{1,0:T(8,128)(2,1)}, u32[]{:S(2)}) copy-start(bf16[192,256]{1,0:T(8,128)(2,1)} %param.17) | copy-start | bytes 294916
  18.8 38.3 %copy-start.6 = (bf16[192,256]{1,0:T(8,128)(2,1)S(1)}, bf16[192,256]{1,0:T(8,128)(2,1)}, u32[]{:S(2)}) copy-start(bf16[192,256]{1,0:T(8,128)(2,1)} %param.16) | copy-start | bytes 294916
  38.9 18.2 %collective-permute-start.1 = (bf16[768,512]{1,0:T(8,128)(2,1)}, bf16[768,512]{1,0:T(8,128)(2,1)}, u32[]{:S(2)}, u32[]{:S(2)}) collective-permute-start(bf16[768,512]{1,0:T(8,128)(2,1)} %bitcast.11), channel_id=1, source_target_pairs={{0,2},{1,3},{2,0},{3,1},{4,6},{5,7},{6,4},{7,5},{8,10},{9,11},{10,... | collective-permute-start | bytes 2359304 | tf_op jit(solution)/shard_map/ppermute | solution.py:66
  40.4 26.0 %all-to-all-start.1 = ((bf16[8,96,512]{2,1,0:T(8,128)(2,1)}), bf16[8,96,512]{2,1,0:T(8,128)(2,1)S(1)}, u32[]{:S(2)}, u32[]{:S(2)}) async-start(bf16[8,96,512]{2,1,0:T(8,128)(2,1)} %bitcast.62), calls=%async_computation.1 | async-start | bytes 1572864 | tf_op jit(solution)/shard_map/all_to_all | solution.py:130
  44.0 18.1 %collective-permute-start = (bf16[768,512]{1,0:T(8,128)(2,1)}, bf16[768,512]{1,0:T(8,128)(2,1)}, u32[]{:S(2)}, u32[]{:S(2)}) collective-permute-start(bf16[768,512]{1,0:T(8,128)(2,1)} %bitcast.11), channel_id=1, source_target_pairs={{0,1},{1,0},{2,3},{3,2},{4,5},{5,4},{6,7},{7,6},{8,9},{9,8},{10,11... | collective-permute-start | bytes 2359304 | tf_op jit(solution)/shard_map/ppermute | solution.py:67
  44.1 13.0 %collective-permute-start.6 = (f32[1,256]{1,0:T(1,128)S(1)}, f32[1,256]{1,0:T(1,128)S(1)}, u32[]{:S(2)}, u32[]{:S(2)}) collective-permute-start(f32[1,256]{1,0:T(1,128)S(1)} %get-tuple-element.28), channel_id=1, source_target_pairs={{0,4},{4,8},{8,12},{12,16},{16,20},{20,24},{24,28},{1,5},{5,9},{9,... | collective-permute-start | bytes 3080 | tf_op jit(solution)/shard_map/ppermute | solution.py:25
  48.0 9.1 %collective-permute-start.7 = (f32[1,256]{1,0:T(1,128)S(1)}, f32[1,256]{1,0:T(1,128)S(1)}, u32[]{:S(2)}, u32[]{:S(2)}) collective-permute-start(f32[1,256]{1,0:T(1,128)S(1)} %get-tuple-element.29), channel_id=1, source_target_pairs={{4,0},{8,4},{12,8},{16,12},{20,16},{24,20},{28,24},{5,1},{9,5},{13... | collective-permute-start | bytes 3080 | tf_op jit(solution)/shard_map/ppermute | solution.py:26
  57.1 11.9 %collective-permute-start.2 = (bf16[768,512]{1,0:T(8,128)(2,1)}, bf16[768,512]{1,0:T(8,128)(2,1)}, u32[]{:S(2)}, u32[]{:S(2)}) collective-permute-start(bf16[768,512]{1,0:T(8,128)(2,1)} %collective-permute-done.1), channel_id=1, source_target_pairs={{0,1},{1,0},{2,3},{3,2},{4,5},{5,4},{6,7},{7,6},{8,9},{9,8},{10,11... | collective-permute-start | bytes 2359304 | tf_op jit(solution)/shard_map/ppermute | solution.py:67
  66.4 23.7 %collective-permute-start.3 = (bf16[768,512]{1,0:T(8,128)(2,1)S(1)}, bf16[768,512]{1,0:T(8,128)(2,1)S(1)}, u32[]{:S(2)}, u32[]{:S(2)}) collective-permute-start(bf16[768,512]{1,0:T(8,128)(2,1)S(1)} %bitcast.59), channel_id=1, source_target_pairs={{0,1},{1,0},{2,3},{3,2},{4,5},{5,4},{6,7},{7,6},{8,9},{9,8},{10,11... | collective-permute-start | bytes 2359304 | tf_op jit(solution)/shard_map/ppermute | solution.py:67
  66.9 19.4 %collective-permute-start.4 = (bf16[768,512]{1,0:T(8,128)(2,1)S(1)}, bf16[768,512]{1,0:T(8,128)(2,1)S(1)}, u32[]{:S(2)}, u32[]{:S(2)}) collective-permute-start(bf16[768,512]{1,0:T(8,128)(2,1)S(1)} %bitcast.60), channel_id=1, source_target_pairs={{0,2},{1,3},{2,0},{3,1},{4,6},{5,7},{6,4},{7,5},{8,10},{9,11},{10,... | collective-permute-start | bytes 2359304 | tf_op jit(solution)/shard_map/ppermute | solution.py:66
  75.0 15.4 %copy-start.12 = (f32[768,512]{1,0:T(8,128)}, f32[768,512]{1,0:T(8,128)S(1)}, u32[]{:S(2)}) copy-start(f32[768,512]{1,0:T(8,128)S(1)} %fusion.1) | copy-start | bytes 4718596
  86.4 3.9 %collective-permute-start.5 = (bf16[768,512]{1,0:T(8,128)(2,1)S(1)}, bf16[768,512]{1,0:T(8,128)(2,1)S(1)}, u32[]{:S(2)}, u32[]{:S(2)}) collective-permute-start(bf16[768,512]{1,0:T(8,128)(2,1)S(1)} %collective-permute-done.4), channel_id=1, source_target_pairs={{0,1},{1,0},{2,3},{3,2},{4,5},{5,4},{6,7},{7,6},{8,9},{9,8},{10,11... | collective-permute-start | bytes 2359304 | tf_op jit(solution)/shard_map/ppermute | solution.py:67
  102.9 2.8 %collective-permute-start.9 = (bf16[768,512]{1,0:T(8,128)(2,1)}, bf16[768,512]{1,0:T(8,128)(2,1)}, u32[]{:S(2)}, u32[]{:S(2)}) collective-permute-start(bf16[768,512]{1,0:T(8,128)(2,1)} %get-tuple-element.19), channel_id=1, source_target_pairs={{0,1},{1,0},{2,3},{3,2},{4,5},{5,4},{6,7},{7,6},{8,9},{9,8},{10,11... | collective-permute-start | bytes 2359304 | tf_op jit(solution)/shard_map/ppermute | solution.py:46
  103.4 6.6 %collective-permute-start.8 = (bf16[768,512]{1,0:T(8,128)(2,1)}, bf16[768,512]{1,0:T(8,128)(2,1)}, u32[]{:S(2)}, u32[]{:S(2)}) collective-permute-start(bf16[768,512]{1,0:T(8,128)(2,1)} %get-tuple-element.18), channel_id=1, source_target_pairs={{0,1},{1,0},{2,3},{3,2},{4,5},{5,4},{6,7},{7,6},{8,9},{9,8},{10,11... | collective-permute-start | bytes 2359304 | tf_op jit(solution)/shard_map/ppermute | solution.py:46
  108.5 20.1 %collective-permute-start.10 = (bf16[768,512]{1,0:T(8,128)(2,1)}, bf16[768,512]{1,0:T(8,128)(2,1)}, u32[]{:S(2)}, u32[]{:S(2)}) collective-permute-start(bf16[768,512]{1,0:T(8,128)(2,1)} %add_convert_fusion.1), channel_id=1, source_target_pairs={{0,2},{1,3},{2,0},{3,1},{4,6},{5,7},{6,4},{7,5},{8,10},{9,11},{10,... | collective-permute-start | bytes 2359304 | tf_op jit(solution)/shard_map/ppermute | solution.py:51
  131.7 35.0 %all-to-all-start.2 = ((bf16[8,96,512]{2,1,0:T(8,128)(2,1)}), bf16[8,96,512]{2,1,0:T(8,128)(2,1)}, u32[]{:S(2)}, u32[]{:S(2)}) async-start(bf16[8,96,512]{2,1,0:T(8,128)(2,1)} %bitcast.23), calls=%async_computation.2 | async-start | bytes 1572864 | tf_op jit(solution)/shard_map/all_to_all | solution.py:130
  141.4 64.8 %all-gather.2.cloned.1.call-start = ((), (), s32[]{:S(2)}) async-start(), calls=%async_computation.4 | async-start | bytes 1769472 | tf_op jit(solution)/shard_map/all_gather | solution.py:156
  178.1 16.2 %collective-permute-start.11 = (f32[1,256]{1,0:T(1,128)S(1)}, f32[1,256]{1,0:T(1,128)S(1)}, u32[]{:S(2)}, u32[]{:S(2)}) collective-permute-start(f32[1,256]{1,0:T(1,128)S(1)} %get-tuple-element.24), channel_id=1, source_target_pairs={{4,0},{8,4},{12,8},{16,12},{20,16},{24,20},{28,24},{5,1},{9,5},{13... | collective-permute-start | bytes 3080 | tf_op jit(solution)/shard_map/ppermute | solution.py:26
  179.4 14.9 %collective-permute-start.12 = (f32[1,256]{1,0:T(1,128)S(1)}, f32[1,256]{1,0:T(1,128)S(1)}, u32[]{:S(2)}, u32[]{:S(2)}) collective-permute-start(f32[1,256]{1,0:T(1,128)S(1)} %get-tuple-element.25), channel_id=1, source_target_pairs={{0,4},{4,8},{8,12},{12,16},{16,20},{20,24},{24,28},{1,5},{5,9},{9,... | collective-permute-start | bytes 3080 | tf_op jit(solution)/shard_map/ppermute | solution.py:25
  184.7 11.5 %all-to-all-start.3 = ((bf16[8,48,256]{2,1,0:T(8,128)(2,1)}), bf16[8,48,256]{2,1,0:T(8,128)(2,1)S(1)}, u32[]{:S(2)}, u32[]{:S(2)}) async-start(bf16[8,48,256]{2,1,0:T(8,128)(2,1)} %copy.24), calls=%async_computation.3 | async-start | bytes 393216 | tf_op jit(solution)/shard_map/all_to_all | solution.py:184
  (8 other events, 24.1 us)
Sparse Core Ops, SparseCore 0:
  144.4 46.1 all-gather.1
